TPU v7x, 32 devices: a whole 2x2x4 slice. The times are simulated.
32 devices in a mesh: ep: 16 (over z, y, x), tp: 2 (over core).
Axes of the slice: x: 2, y: 2, z: 4, core: 2. Of those that a mesh axis runs over, the one named last changes fastest.
Arguments:
- tokens: bfloat16 [256, 2048], P('ep'), may hold values from -6 to 6
- lengths: int32 [256], P('ep'), may hold values from 1 to 1024, as said below
- attn_gain: float32 [2048], replicated, may hold values from 0.1 to 1.9
- w_query: bfloat16 [2048, 1024], P(None, 'tp'), may hold values from -0.125 to 0.125
- w_key: bfloat16 [2048, 128], P(None, 'tp'), may hold values from -0.125 to 0.125
- w_value: bfloat16 [2048, 128], P(None, 'tp'), may hold values from -0.125 to 0.125
- head_bias: float32 [16], P('tp'), may hold values from -7 to -2
- key_cache: bfloat16 [256, 2, 64, 1024], P('ep', 'tp'), may hold values from -6 to 6
- value_cache: bfloat16 [256, 2, 64, 1024], P('ep', 'tp'), may hold values from -6 to 6
- w_attn_out: bfloat16 [1024, 2048], P('tp'), may hold values from -0.1875 to 0.1875
- ffn_gain: float32 [2048], replicated, may hold values from 0.1 to 1.9
- w_router: bfloat16 [2048, 16], replicated, may hold values from -0.125 to 0.125
- routes: int32 [256, 6], P('ep'), may hold values from 0 to 15, all different within a row; in each aligned block of 16 rows (0 to 15, 16 to 31, ...) at most 12 rows name the same one
- w_dense_gate: bfloat16 [2048, 512], P('ep', 'tp'), may hold values from -0.125 to 0.125
- w_dense_up: bfloat16 [2048, 512], P('ep', 'tp'), may hold values from -0.125 to 0.125
- w_dense_down: bfloat16 [512, 2048], P('tp', 'ep'), may hold values from -0.25 to 0.25
- dense_mix: float32 [2048], replicated, may hold values from -0.125 to 0.125
- w_expert_gate: bfloat16 [16, 2048, 512], P('ep', None, 'tp'), may hold values from -0.125 to 0.125
- w_expert_up: bfloat16 [16, 2048, 512], P('ep', None, 'tp'), may hold values from -0.125 to 0.125
- w_expert_down: bfloat16 [16, 512, 2048], P('ep', 'tp'), may hold values from -0.25 to 0.25
Outputs:
- layer_out: bfloat16 [256, 2048], P('ep', 'tp')
- new_keys: bfloat16 [256, 128], P('ep', 'tp')
- new_values: bfloat16 [256, 128], P('ep', 'tp')
Inputs may be any that keep to these rules, and one draw needn't show every extreme that they name: `lengths`: every sequence holds between 1 and 1024 cached positions; in every draw some sequence holds exactly 1024. `routes`: each token names 6 different experts. Among the rows of one device no expert is named by more than 12 rows.
All inputs are finite; a program needn't handle non-finite values.
Results may differ from a plain program's by a relative error of at most 0.014.
Values may be sent and summed in bfloat16 or wider, within the bound.
A program may use at most 64 MiB of HBM per device.

v0:
```python
import jax
import jax.numpy as jnp
from jax import lax
from jax.sharding import PartitionSpec as P


def rms_scale(values, gain):
    wide = values.astype(jnp.float32)
    return wide * lax.rsqrt(jnp.mean(wide * wide, axis=-1, keepdims=True) + 1e-06) * gain


def stick_read(queries, lengths, head_bias, key_cache, value_cache):
    seq_count, local_kv, head_dim, cache_len = key_cache.shape
    group_size = head_bias.shape[0] // local_kv
    grouped = queries.reshape(seq_count, local_kv, group_size, head_dim)
    head_shift = head_bias.reshape(1, local_kv, group_size, 1)
    span_len = min(512, cache_len)
    block_count = (jnp.max(lengths) + span_len - 1) // span_len
    span_index = lax.iota(jnp.int32, span_len)
    after_mask = (span_index[:, None] > span_index[None, :]).astype(jnp.float32)

    def visit(visit_index, carry):
        totals, log_later = carry
        first = (block_count - 1 - visit_index) * span_len
        key_block = lax.dynamic_slice_in_dim(key_cache, first, span_len, 3)
        value_block = lax.dynamic_slice_in_dim(value_cache, first, span_len, 3)
        scores = (
            jnp.einsum("skgd,skdc->skgc", grouped, key_block, preferred_element_type=jnp.float32)
            * head_dim ** (-0.5)
            + head_shift
        )
        positions = first + span_index
        visible = (positions[None, :] < lengths[:, None])[:, None, None, :]
        log_keep = jnp.where(visible, jax.nn.log_sigmoid(-scores), 0.0)
        log_after = (
            jnp.einsum("skgj,jc->skgc", log_keep, after_mask, precision=lax.Precision.HIGHEST)
            + log_later[..., None]
        )
        weights = jnp.where(visible, jnp.exp(jax.nn.log_sigmoid(scores) + log_after), 0.0).astype(
            jnp.bfloat16
        )
        totals = totals + jnp.einsum(
            "skgc,skdc->skgd", weights, value_block, preferred_element_type=jnp.float32
        )
        return (totals, log_later + jnp.sum(log_keep, axis=3))

    start_totals = jnp.zeros((seq_count, local_kv, group_size, head_dim), jnp.float32)
    start_later = jnp.zeros((seq_count, local_kv, group_size), jnp.float32)
    totals, unused_later = lax.fori_loop(0, block_count, visit, (start_totals, start_later))
    return totals.reshape(seq_count, -1).astype(jnp.bfloat16)


def expert_math(inputs, w_expert_gate, w_expert_up, w_expert_down):
    gate_rows = jnp.einsum(
        "njcd,jdf->njcf", inputs, w_expert_gate, preferred_element_type=jnp.float32
    )
    up_rows = jnp.einsum("njcd,jdf->njcf", inputs, w_expert_up, preferred_element_type=jnp.float32)
    hidden = (jax.nn.silu(gate_rows) * up_rows).astype(jnp.bfloat16)
    partial_value = jnp.einsum(
        "njcf,jfd->njcd", hidden, w_expert_down, preferred_element_type=jnp.float32
    ).astype(jnp.bfloat16)
    return (
        lax.psum_scatter(partial_value, "tp", scatter_dimension=3, tiled=True)
        .astype(jnp.float32)
        .astype(jnp.bfloat16)
    )


def shards(
    tokens,
    lengths,
    attn_gain,
    w_query,
    w_key,
    w_value,
    head_bias,
    key_cache,
    value_cache,
    w_attn_out,
    ffn_gain,
    w_router,
    routes,
    w_dense_gate,
    w_dense_up,
    w_dense_down,
    dense_mix,
    w_expert_gate,
    w_expert_up,
    w_expert_down,
):
    seq_count, model_width = tokens.shape
    normed = rms_scale(tokens, attn_gain).astype(jnp.bfloat16)
    new_keys = jnp.dot(normed, w_key, preferred_element_type=jnp.float32).astype(jnp.bfloat16)
    new_values = jnp.dot(normed, w_value, preferred_element_type=jnp.float32).astype(jnp.bfloat16)
    queries = jnp.dot(normed, w_query, preferred_element_type=jnp.float32).astype(jnp.bfloat16)
    heads_out = stick_read(queries, lengths, head_bias, key_cache, value_cache)
    attn_partial = jnp.dot(heads_out, w_attn_out, preferred_element_type=jnp.float32).astype(
        jnp.bfloat16
    )
    attn = lax.psum(attn_partial, "tp").astype(jnp.float32)
    residual = (tokens.astype(jnp.float32) + attn).astype(jnp.bfloat16)
    normed2 = rms_scale(residual, ffn_gain).astype(jnp.bfloat16)
    expert_total = w_router.shape[1]
    top_count = routes.shape[1]
    probs = jax.nn.sigmoid(jnp.dot(normed2, w_router, preferred_element_type=jnp.float32))
    hits = routes[:, :, None] == lax.iota(jnp.int32, expert_total)[None, None, :]
    picked = jnp.sum(jnp.where(hits, probs[:, None, :], 0.0), axis=-1)
    gates = picked / jnp.sum(picked, axis=-1, keepdims=True) * 2.5
    capacity = max(2, 2 * seq_count * top_count // expert_total)
    slot_total = expert_total * capacity
    flat_routes = routes.reshape(-1)
    route_count = flat_routes.shape[0]
    matching = flat_routes[:, None] == flat_routes[None, :]
    earlier = lax.iota(jnp.int32, route_count)[:, None] > lax.iota(jnp.int32, route_count)[None, :]
    slot_rank = jnp.sum(jnp.logical_and(matching, earlier).astype(jnp.int32), axis=1)
    target = flat_routes * capacity + slot_rank
    one_hot = (target[:, None] == lax.iota(jnp.int32, slot_total)[None, :]).astype(jnp.bfloat16)
    dispatch = jnp.sum(one_hot.reshape(seq_count, top_count, slot_total), axis=1)
    send_rows = jnp.einsum(
        "sr,sd->rd", dispatch, normed2, preferred_element_type=jnp.float32
    ).astype(jnp.bfloat16)
    send_rows = send_rows.reshape(expert_total, capacity, model_width)
    local_experts = w_expert_gate.shape[0]
    received = lax.all_to_all(send_rows, "ep", split_axis=0, concat_axis=0, tiled=True)
    source_count = received.shape[0] // local_experts
    item_count = received.shape[1]
    inputs = received.reshape(source_count, local_experts, item_count, model_width)
    summed = expert_math(inputs, w_expert_gate, w_expert_up, w_expert_down)
    summed = summed.reshape(source_count * local_experts, item_count, summed.shape[3])
    returned = lax.all_to_all(summed, "ep", split_axis=0, concat_axis=0, tiled=True)
    half_width = returned.shape[2]
    route_rows = returned.reshape(slot_total, half_width)[target]
    route_rows = route_rows.reshape(seq_count, top_count, half_width)
    routed = jnp.sum(gates[:, :, None] * route_rows.astype(jnp.float32), axis=1)
    features2 = lax.all_to_all(normed2, "ep", split_axis=1, concat_axis=0, tiled=True)
    paired_weights = jnp.concatenate([w_dense_gate, w_dense_up], axis=1)
    paired = lax.psum_scatter(
        jnp.dot(features2, paired_weights, preferred_element_type=jnp.float32),
        "ep",
        scatter_dimension=0,
        tiled=True,
    )
    hidden_cols = w_dense_gate.shape[1]
    dense_gate_rows = paired[:, :hidden_cols]
    dense_up_rows = paired[:, hidden_cols:]
    dense_hidden = (jax.nn.silu(dense_gate_rows) * dense_up_rows).astype(jnp.bfloat16)
    dense_columns = jnp.dot(
        lax.all_gather(dense_hidden, "ep", axis=0, tiled=True),
        w_dense_down,
        preferred_element_type=jnp.float32,
    )
    dense_partial = lax.all_to_all(
        dense_columns.astype(jnp.bfloat16), "ep", split_axis=0, concat_axis=1, tiled=True
    )
    dense = lax.psum_scatter(dense_partial, "tp", scatter_dimension=1, tiled=True).astype(
        jnp.float32
    )
    mix_gate = jax.nn.sigmoid(jnp.sum(normed2.astype(jnp.float32) * dense_mix, axis=-1))
    offset = lax.axis_index("tp") * half_width
    residual_half = lax.dynamic_slice_in_dim(residual, offset, half_width, 1)
    layer_out = (residual_half.astype(jnp.float32) + mix_gate[:, None] * dense + routed).astype(
        jnp.bfloat16
    )
    return (layer_out, new_keys, new_values)


def solution(mesh):
    return jax.shard_map(
        shards,
        mesh=mesh,
        in_specs=(
            P("ep", None),
            P("ep"),
            P(),
            P(None, "tp"),
            P(None, "tp"),
            P(None, "tp"),
            P("tp"),
            P("ep", "tp", None, None),
            P("ep", "tp", None, None),
            P("tp", None),
            P(),
            P(),
            P("ep", None),
            P("ep", "tp"),
            P("ep", "tp"),
            P("tp", "ep"),
            P(),
            P("ep", None, "tp"),
            P("ep", None, "tp"),
            P("ep", "tp", None),
        ),
        out_specs=(P("ep", "tp"), P("ep", "tp"), P("ep", "tp")),
        check_vma=False,
    )
```

profile of v0, /device:TPU:0, one launch (start us, length us, event | category | flops | bytes accessed | tf_op | source)
XLA Modules:
  0.0 217.0 jit_solution(16179048854171437925)
XLA Ops:
  7.2 0.0 all-reduce.2.cloned.1.call-start
  7.2 1.4 reduce_max.9
  9.3 1.0 fusion.40
  10.3 2.1 convolution_convert_fusion.4
  12.4 0.1 reshape.238
  12.5 3.9 %while.15 = (s32[]{:T(128)}, f32[16,1,8,64]{3,2,0,1:T(8,128)S(1)}, f32[16,1,8]{0,2,1:T(8,128)S(1)}, s32[]{:T(128)}, s32[]{:T(128)}, /*index=5*/s32[16]{0:T(128)S...) while((s32[]{:T(128)}, f32[16,1,8,64]{3,2,0,1:T(8,128)S(1)}, ...), condition=%wide.region_4.5_spmd.clone, body=%wide.region_2.4_spmd.clone.sunk | while | flops 422003200 | bytes 11420487 | solution.py:49
  12.6 0.1 broadcast_compare_fusion.2
  12.7 1.6 fusion.88
  14.3 0.1 copy.74
  14.4 0.9 fusion.89
  15.3 0.7 copy-done.1
  16.0 0.4 fusion.90
  16.3 0.1 copy.75
  16.4 0.0 copy-start.7
  16.5 0.1 convert_element_type.104
  16.6 1.0 convolution_convert_fusion.2
  17.6 0.0 all-reduce.2.cloned.1.call-update
  17.6 0.1 copy.60
  17.7 0.1 eq.45
  17.8 0.2 convert_reduce_fusion
  18.0 0.1 reduce_sum.96
  18.1 0.1 copy.62
  18.2 0.1 fusion.50
  18.3 23.8 %all-reduce.2.cloned.1.call-done = bf16[16,2048]{1,0:T(8,128)(2,1)} async-done(((bf16[16,2048]{1,0:T(8,128)(2,1)}), bf16[16,2048]{1,0:T(8,128)(2,1)}) %all-reduce.2.cloned.1.call-update) | async-done | bytes 65552 | tf_op jit(solution)/shard_map/psum | solution.py:100
  42.1 1.0 fusion.37
  43.1 0.2 multiply_reduce_fusion.1
  43.3 0.6 copy.71
  43.9 6.8 %all-to-all-start = ((bf16[16,16,128]{2,0,1:T(8,128)(2,1)}), bf16[16,16,128]{2,0,1:T(8,128)(2,1)S(1)}, u32[]{:S(2)}, u32[]{:S(2)}) async-start(bf16[16,16,128]{2,0,1:T(8,128)(2,1)} %bitcast.105), calls=%async_computation | async-start | bytes 131072 | tf_op jit(solution)/shard_map/all_to_all | solution.py:135
  50.8 0.4 convolution_convert_fusion.1
  51.2 1.2 reshape.240
  52.3 5.9 %all-to-all-done = bf16[16,16,128]{2,0,1:T(8,128)(2,1)S(1)} async-done(((bf16[16,16,128]{2,0,1:T(8,128)(2,1)}), bf16[16,16,128]{2,0,1:T(8,128)(2,1)S(1)}, u32[]{:S(2)}, u32[]{:S(2)}) %all-to-all-start) | async-done | bytes 65568 | tf_op jit(solution)/shard_map/all_to_all | solution.py:135
  58.3 3.7 %all-to-all-start.2 = ((bf16[16,12,2048]{2,1,0:T(8,128)(2,1)}), bf16[16,12,2048]{2,1,0:T(8,128)(2,1)S(1)}, u32[]{:S(2)}, u32[]{:S(2)}) async-start(bf16[16,12,2048]{2,1,0:T(8,128)(2,1)} %reshape.240), calls=%async_computation.4 | async-start | bytes 2097152 | tf_op jit(solution)/shard_map/all_to_all | solution.py:124
  62.0 0.0 reduce-scatter.4.cloned.1.call-start
  62.0 1.0 fusion.44
  63.1 0.0 reduce-scatter.4.cloned.1.call-update
  63.1 0.0 reduce-scatter.8.cloned.1.call-start
  63.1 0.1 mul.144
  63.2 23.2 %all-to-all-done.2 = bf16[16,12,2048]{2,1,0:T(8,128)(2,1)S(1)} async-done(((bf16[16,12,2048]{2,1,0:T(8,128)(2,1)}), bf16[16,12,2048]{2,1,0:T(8,128)(2,1)S(1)}, u32[]{:S(2)}, u32[]{:S(2)}) %all-to-all-start.2) | async-done | bytes 786464 | tf_op jit(solution)/shard_map/all_to_all | solution.py:124
  86.4 1.7 convolution_bitcast_fusion.2
  88.2 0.4 fusion.30
  88.7 0.8 copy-done.2
  89.5 1.3 fusion.27
  90.8 0.8 convolution_convert_fusion.5
  91.6 0.8 convolution_convert_fusion.6
  92.5 51.5 %reduce-scatter.4.cloned.1.call-done = f32[16,512]{1,0:T(8,128)} async-done(((f32[256,512]{1,0:T(8,128)}), f32[16,512]{1,0:T(8,128)}) %reduce-scatter.4.cloned.1.call-update) | async-done | bytes 32784 | tf_op jit(solution)/shard_map/reduce_scatter | solution.py:137
  144.0 0.7 fusion.52
  144.7 37.0 %all_gather.3 = bf16[256,256]{1,0:T(8,128)(2,1)S(1)} all-gather(bf16[16,256]{1,0:T(8,128)(2,1)S(1)} %fusion.52), channel_id=1, replica_groups=mesh['ep'=16,'tp'=2] {'ep'}, dimensions={0}, use_global_device_ids=true | all-gather | bytes 139264 | tf_op jit(solution)/shard_map/all_gather | solution.py:148
  181.7 0.8 convolution_convert_fusion.3
  182.5 3.5 %all-to-all-start.1 = ((bf16[16,16,128]{2,1,0:T(8,128)(2,1)}), bf16[16,16,128]{2,1,0:T(8,128)(2,1)S(1)}, u32[]{:S(2)}, u32[]{:S(2)}) async-start(bf16[16,16,128]{2,1,0:T(8,128)(2,1)} %bitcast.5), calls=%async_computation.2 | async-start | bytes 131072 | tf_op jit(solution)/shard_map/all_to_all | solution.py:152
  186.0 0.2 fusion.33
  186.2 0.2 select_reduce_fusion
  186.5 2.0 copy.64
  188.5 5.0 %all-to-all-done.1 = bf16[16,16,128]{2,1,0:T(8,128)(2,1)S(1)} async-done(((bf16[16,16,128]{2,1,0:T(8,128)(2,1)}), bf16[16,16,128]{2,1,0:T(8,128)(2,1)S(1)}, u32[]{:S(2)}, u32[]{:S(2)}) %all-to-all-start.1) | async-done | bytes 65568 | tf_op jit(solution)/shard_map/all_to_all | solution.py:152
  193.5 3.6 %all-to-all-start.3 = ((bf16[16,12,1024]{2,1,0:T(8,128)(2,1)}), bf16[16,12,1024]{2,1,0:T(8,128)(2,1)S(1)}, u32[]{:S(2)}, u32[]{:S(2)}) async-start(bf16[16,12,1024]{2,1,0:T(8,128)(2,1)} %copy.64), calls=%async_computation.6 | async-start | bytes 1048576 | tf_op jit(solution)/shard_map/all_to_all | solution.py:130
  197.1 0.0 reduce-scatter.6.cloned.1.call-start
  197.1 0.1 copy.59
  197.2 0.6 copy_bitcast_fusion
  197.9 9.9 %all-to-all-done.3 = bf16[16,12,1024]{2,1,0:T(8,128)(2,1)S(1)} async-done(((bf16[16,12,1024]{2,1,0:T(8,128)(2,1)}), bf16[16,12,1024]{2,1,0:T(8,128)(2,1)S(1)}, u32[]{:S(2)}, u32[]{:S(2)}) %all-to-all-start.3) | async-done | bytes 393248 | tf_op jit(solution)/shard_map/all_to_all | solution.py:130
  207.8 0.1 reshape.246
  207.9 0.8 gather_fusion
  208.7 0.1 reshape.247
  208.7 0.2 multiply_reduce_fusion
  209.0 0.0 reduce-scatter.6.cloned.1.call-done
  209.0 1.5 add_convert_fusion
  (46 shorter events, 0.2 us)
Async XLA Ops:
  7.2 9.4 %copy-start = (bf16[512,2048]{1,0:T(8,128)(2,1)S(1)}, bf16[512,2048]{1,0:T(8,128)(2,1)}, u32[]{:S(2)}) copy-start(bf16[512,2048]{1,0:T(8,128)(2,1)} %param.31) | copy-start | bytes 6291460
  7.2 5.3 %copy-start.9 = (s32[16]{0:T(128)S(1)}, s32[16]{0:T(128)}, u32[]{:S(2)}) copy-start(s32[16]{0:T(128)} %param.23) | copy-start | bytes 196
  7.2 5.3 %copy-start.16 = (f32[8]{0:T(128)S(1)}, f32[8]{0:T(128)}, u32[]{:S(2)}) copy-start(f32[8]{0:T(128)} %param.28) | copy-start | bytes 100
  7.2 34.9 %all-reduce.2.cloned.1.call-start = ((), (), s32[]{:S(2)}) async-start(), calls=%async_computation.7 | async-start | bytes 131072 | tf_op jit(solution)/shard_map/psum | solution.py:100
  14.4 1.6 copy-start.1
  16.4 1.2 copy-start.8
  16.4 25.7 %copy-start.3 = (bf16[16,2048]{1,0:T(8,128)(2,1)S(1)}, bf16[16,2048]{1,0:T(8,128)(2,1)}, u32[]{:S(2)}) copy-start(bf16[16,2048]{1,0:T(8,128)(2,1)} %param.22) | copy-start | bytes 196612
  16.4 26.6 %copy-start.7 = (f32[2048]{0:T(1024)S(1)}, f32[2048]{0:T(1024)}, u32[]{:S(2)}) copy-start(f32[2048]{0:T(1024)} %param.32) | copy-start | bytes 24580
  16.4 26.6 %copy-start.11 = (f32[2048]{0:T(1024)S(1)}, f32[2048]{0:T(1024)}, u32[]{:S(2)}) copy-start(f32[2048]{0:T(1024)} %param.38) | copy-start | bytes 24580
  43.9 14.4 %all-to-all-start = ((bf16[16,16,128]{2,0,1:T(8,128)(2,1)}), bf16[16,16,128]{2,0,1:T(8,128)(2,1)S(1)}, u32[]{:S(2)}, u32[]{:S(2)}) async-start(bf16[16,16,128]{2,0,1:T(8,128)(2,1)} %bitcast.105), calls=%async_computation | async-start | bytes 131072 | tf_op jit(solution)/shard_map/all_to_all | solution.py:135
  51.2 10.8 %copy-start.5 = (bf16[128,256]{1,0:T(8,128)(2,1)S(1)}, bf16[128,256]{1,0:T(8,128)(2,1)}, u32[]{:S(2)}) copy-start(bf16[128,256]{1,0:T(8,128)(2,1)} %param.36) | copy-start | bytes 196612
  51.2 10.8 %copy-start.6 = (bf16[128,256]{1,0:T(8,128)(2,1)S(1)}, bf16[128,256]{1,0:T(8,128)(2,1)}, u32[]{:S(2)}) copy-start(bf16[128,256]{1,0:T(8,128)(2,1)} %param.35) | copy-start | bytes 196612
  58.3 28.1 %all-to-all-start.2 = ((bf16[16,12,2048]{2,1,0:T(8,128)(2,1)}), bf16[16,12,2048]{2,1,0:T(8,128)(2,1)S(1)}, u32[]{:S(2)}, u32[]{:S(2)}) async-start(bf16[16,12,2048]{2,1,0:T(8,128)(2,1)} %reshape.240), calls=%async_computation.4 | async-start | bytes 2097152 | tf_op jit(solution)/shard_map/all_to_all | solution.py:124
  62.0 82.0 %reduce-scatter.4.cloned.1.call-start = ((), (), s32[]{:S(2)}) async-start(), calls=%async_computation.8 | async-start | bytes 557056 | tf_op jit(solution)/shard_map/reduce_scatter | solution.py:137
  63.1 123.4 %reduce-scatter.8.cloned.1.call-start = ((), (), s32[]{:S(2)}) async-start(), calls=%async_computation.10 | async-start | bytes 1179648 | tf_op jit(solution)/shard_map/reduce_scatter | solution.py:63
  86.4 1.8 copy-start.12
  88.2 1.2 copy-start.2
  89.4 1.3 copy-start.10
  89.4 1.3 copy-start.13
  89.4 2.2 %copy-start.14 = (bf16[2048,64]{0,1:T(8,128)(2,1)S(1)}, bf16[2048,64]{0,1:T(8,128)(2,1)}, u32[]{:S(2)}) copy-start(bf16[2048,64]{0,1:T(8,128)(2,1)} %param.26) | copy-start | bytes 786436
  89.5 92.3 %copy-start.4 = (bf16[256,128]{1,0:T(8,128)(2,1)S(1)}, bf16[256,128]{1,0:T(8,128)(2,1)}, u32[]{:S(2)}) copy-start(bf16[256,128]{1,0:T(8,128)(2,1)} %param.37) | copy-start | bytes 196612
  89.5 96.5 %copy-start.15 = (bf16[2048,16]{0,1:T(8,128)(2,1)S(1)}, bf16[2048,16]{0,1:T(8,128)(2,1)}, u32[]{:S(2)}) copy-start(bf16[2048,16]{0,1:T(8,128)(2,1)} %param.33) | copy-start | bytes 196612
  182.5 11.0 %all-to-all-start.1 = ((bf16[16,16,128]{2,1,0:T(8,128)(2,1)}), bf16[16,16,128]{2,1,0:T(8,128)(2,1)S(1)}, u32[]{:S(2)}, u32[]{:S(2)}) async-start(bf16[16,16,128]{2,1,0:T(8,128)(2,1)} %bitcast.5), calls=%async_computation.2 | async-start | bytes 131072 | tf_op jit(solution)/shard_map/all_to_all | solution.py:152
  193.5 14.3 %all-to-all-start.3 = ((bf16[16,12,1024]{2,1,0:T(8,128)(2,1)}), bf16[16,12,1024]{2,1,0:T(8,128)(2,1)S(1)}, u32[]{:S(2)}, u32[]{:S(2)}) async-start(bf16[16,12,1024]{2,1,0:T(8,128)(2,1)} %copy.64), calls=%async_computation.6 | async-start | bytes 1048576 | tf_op jit(solution)/shard_map/all_to_all | solution.py:130
  197.1 11.9 %reduce-scatter.6.cloned.1.call-start = ((), (), s32[]{:S(2)}) async-start(), calls=%async_computation.9 | async-start | bytes 98304 | tf_op jit(solution)/shard_map/reduce_scatter | solution.py:155
Sparse Core Ops, SparseCore 0:
  17.7 24.2 all-reduce.1
  65.0 78.8 reduce-scatter.3
  146.2 4.7 reduce-scatter.7
  199.8 8.7 reduce-scatter.5
where the time goes:
time: 218 us; the launch traced here: 217 us
  waiting for transfers between devices  119 us (55%)
  blocking collectives  37 us (17%)
  starting transfers between devices  17.7 us (8%)
  between operations  14.8 us (7%)
  matrix products  13.6 us (6%)
  local copies, waits for them, and re-layouts  7.75 us (4%)
  other arithmetic  6.66 us (3%)
    reduce_scatter x1, waiting for transfers between devices, shards(): lax.psum_scatter(jnp.dot(features2, paired_weights, preferred_element_typ...  51.5 us
    all_gather x1, blocking collectives, shards(): lax.all_gather(dense_hidden, 'ep', axis=0, tiled=True)  37 us
    psum x1, waiting for transfers between devices, shards(): attn = lax.psum(attn_partial, 'tp').astype(jnp.float32)  23.8 us
    all_to_all x1, waiting for transfers between devices, shards(): lax.all_to_all(send_rows, 'ep', split_axis=0, concat_axis=0, tiled=True)  23.2 us
    all_to_all x1, waiting for transfers between devices, shards(): lax.all_to_all(summed, 'ep', split_axis=0, concat_axis=0, tiled=True)  9.93 us
    all_to_all x1, starting transfers between devices, shards(): lax.all_to_all(normed2, 'ep', split_axis=1, concat_axis=0, tiled=True)  6.83 us
    all_to_all x1, waiting for transfers between devices, shards(): lax.all_to_all(normed2, 'ep', split_axis=1, concat_axis=0, tiled=True)  5.95 us
    all_to_all x1, waiting for transfers between devices, shards(): lax.all_to_all(dense_columns.astype(jnp.bfloat16), 'ep', split_axis=0, co...  5.01 us
  transfers between devices with their start and end apart: 8, of which 6 were waited for; matrix products, arithmetic and copies ran while one was open for 7% of the time, Pallas kernels for 0%

commit v1 on v0

--- a/solution.py
+++ b/solution.py
@@ -2,6 +2,11 @@
 import jax.numpy as jnp
 from jax import lax
 from jax.sharding import PartitionSpec as P
+
+
+def summed_here(shard, name):
+    parts = lax.all_gather(shard, name)
+    return jnp.sum(parts, axis=0)
 
 
 def rms_scale(values, gain):
@@ -97,7 +102,7 @@
     attn_partial = jnp.dot(heads_out, w_attn_out, preferred_element_type=jnp.float32).astype(
         jnp.bfloat16
     )
-    attn = lax.psum(attn_partial, "tp").astype(jnp.float32)
+    attn = summed_here(attn_partial, "tp").astype(jnp.float32)
     residual = (tokens.astype(jnp.float32) + attn).astype(jnp.bfloat16)
     normed2 = rms_scale(residual, ffn_gain).astype(jnp.bfloat16)
     expert_total = w_router.shape[1]

time: 218 us -> 199 us (0.913)
  waiting for transfers between devices: 119 us -> 95 us
  starting transfers between devices: 17.7 us -> 22.9 us
    psum x1 -> x0, waiting for transfers between devices: 23.8 us -> none  [shards(): attn = lax.psum(attn_partial, 'tp').astype(jnp.float32)]
    all_to_all x1, starting transfers between devices: 6.83 us -> 12.1 us  [shards(): lax.all_to_all(normed2, 'ep', split_axis=1, concat_axis=0, tiled=True)]
  transfers between devices with their start and end apart: 8 -> 7, of which waited for: 6 -> 5; matrix products, arithmetic and copies ran while one was open for 7% -> 7% of each run, Pallas kernels for 0% -> 0%
where the time goes in v1:
time: 199 us; the launch traced here: 198 us
  waiting for transfers between devices  95 us (48%)
  blocking collectives  39 us (20%)
  starting transfers between devices  22.9 us (12%)
  between operations  14.8 us (7%)
  matrix products  13 us (7%)
  local copies, waits for them, and re-layouts  7.75 us (4%)
  other arithmetic  5.84 us (3%)
    reduce_scatter x1, waiting for transfers between devices, shards(): lax.psum_scatter(jnp.dot(features2, paired_weights, preferred_element_typ...  51.7 us
    all_gather x1, blocking collectives, shards(): lax.all_gather(dense_hidden, 'ep', axis=0, tiled=True)  37 us
    all_to_all x1, waiting for transfers between devices, shards(): lax.all_to_all(send_rows, 'ep', split_axis=0, concat_axis=0, tiled=True)  23.3 us
    all_to_all x1, starting transfers between devices, shards(): lax.all_to_all(normed2, 'ep', split_axis=1, concat_axis=0, tiled=True)  12.1 us
    all_to_all x1, waiting for transfers between devices, shards(): lax.all_to_all(summed, 'ep', split_axis=0, concat_axis=0, tiled=True)  9.1 us
    all_to_all x1, waiting for transfers between devices, shards(): lax.all_to_all(dense_columns.astype(jnp.bfloat16), 'ep', split_axis=0, co...  5.43 us
    all_to_all x1, waiting for transfers between devices, shards(): lax.all_to_all(normed2, 'ep', split_axis=1, concat_axis=0, tiled=True)  5.28 us
  transfers between devices with their start and end apart: 7, of which 5 were waited for; matrix products, arithmetic and copies ran while one was open for 7% of the time, Pallas kernels for 0%

profile of v1, /device:TPU:0, one launch (start us, length us, event | category | flops | bytes accessed | tf_op | source)
XLA Modules:
  0.0 198.3 jit_solution(2389787002278691970)
XLA Ops:
  7.2 1.4 reduce_max.9
  9.3 1.0 fusion.40
  10.3 2.1 %convolution_convert_fusion.4 = bf16[16,512]{1,0:T(8,128)(2,1)S(1)} fusion(bf16[2048,512]{1,0:T(8,128)(2,1)} %param.25, bf16[16,2048]{1,0:T(8,128)(2,1)} %param.22, f32[2048]{0:T(1024)} %param.24, f32[16]{0:T(128)S(1)} %add_rsqrt_fusion.1), kind=kOutput, calls=%fused_computation.44 | convolution fusion | flops 33693696 | bytes 2187328 | tf_op jit(solution)/shard_map/dot_general | solution.py:100
  12.4 0.1 reshape.238
  12.5 3.9 %while.15 = (s32[]{:T(128)}, f32[16,1,8,64]{3,2,0,1:T(8,128)S(1)}, f32[16,1,8]{0,2,1:T(8,128)S(1)}, s32[]{:T(128)}, s32[]{:T(128)}, /*index=5*/s32[16]{0:T(128)S...) while((s32[]{:T(128)}, f32[16,1,8,64]{3,2,0,1:T(8,128)S(1)}, ...), condition=%wide.region_4.5_spmd.clone, body=%wide.region_2.4_spmd.clone.sunk | while | flops 422003200 | bytes 11420487 | solution.py:54
  12.6 0.1 broadcast_compare_fusion.2
  12.6 1.6 fusion.88
  14.3 0.1 copy.83
  14.3 0.9 fusion.89
  15.3 0.7 copy-done.1
  15.9 0.4 fusion.90
  16.3 0.1 copy.84
  16.4 0.0 copy-start.11
  16.4 0.1 convert_element_type.106
  16.5 0.4 convolution_convert_fusion.2
  16.9 2.0 %all-gather = bf16[32,2048]{1,0:T(8,128)(2,1)S(1)} all-gather(bf16[16,2048]{1,0:T(8,128)(2,1)S(1)} %convolution_convert_fusion.2), channel_id=2, replica_groups=mesh['ep'=16,'tp'=2] {'tp'}, dimensions={0}, use_global_device_ids=true | all-gather | bytes 196608 | tf_op jit(solution)/shard_map/all_gather | solution.py:8
  19.0 0.1 fusion.37
  19.2 0.2 multiply_reduce_fusion.1
  19.4 0.6 copy.80
  20.0 12.1 %all-to-all-start = ((bf16[16,16,128]{2,0,1:T(8,128)(2,1)}), bf16[16,16,128]{2,0,1:T(8,128)(2,1)S(1)}, u32[]{:S(2)}, u32[]{:S(2)}) async-start(bf16[16,16,128]{2,0,1:T(8,128)(2,1)} %bitcast.106), calls=%async_computation | async-start | bytes 131072 | tf_op jit(solution)/shard_map/all_to_all | solution.py:140
  32.1 0.1 copy.69
  32.2 0.1 eq.45
  32.3 0.2 convert_reduce_fusion
  32.4 0.1 reduce_sum.109
  32.5 0.1 copy.71
  32.6 0.1 fusion.50
  32.7 0.4 convolution_convert_fusion.1
  33.2 1.2 reshape.240
  34.3 5.3 %all-to-all-done = bf16[16,16,128]{2,0,1:T(8,128)(2,1)S(1)} async-done(((bf16[16,16,128]{2,0,1:T(8,128)(2,1)}), bf16[16,16,128]{2,0,1:T(8,128)(2,1)S(1)}, u32[]{:S(2)}, u32[]{:S(2)}) %all-to-all-start) | async-done | bytes 65568 | tf_op jit(solution)/shard_map/all_to_all | solution.py:140
  39.6 3.7 %all-to-all-start.2 = ((bf16[16,12,2048]{2,1,0:T(8,128)(2,1)}), bf16[16,12,2048]{2,1,0:T(8,128)(2,1)S(1)}, u32[]{:S(2)}, u32[]{:S(2)}) async-start(bf16[16,12,2048]{2,1,0:T(8,128)(2,1)} %reshape.240), calls=%async_computation.4 | async-start | bytes 2097152 | tf_op jit(solution)/shard_map/all_to_all | solution.py:129
  43.3 0.0 reduce-scatter.4.cloned.1.call-start
  43.3 1.0 fusion.44
  44.4 0.0 reduce-scatter.4.cloned.1.call-update
  44.4 0.0 reduce-scatter.8.cloned.1.call-start
  44.4 23.3 %all-to-all-done.2 = bf16[16,12,2048]{2,1,0:T(8,128)(2,1)S(1)} async-done(((bf16[16,12,2048]{2,1,0:T(8,128)(2,1)}), bf16[16,12,2048]{2,1,0:T(8,128)(2,1)S(1)}, u32[]{:S(2)}, u32[]{:S(2)}) %all-to-all-start.2) | async-done | bytes 786464 | tf_op jit(solution)/shard_map/all_to_all | solution.py:129
  67.8 1.8 convolution_bitcast_fusion.2
  69.6 0.5 fusion.30
  70.0 0.8 copy-done.2
  70.8 1.3 fusion.27
  72.1 0.0 reduce-scatter.8.cloned.1.call-update
  72.1 0.2 fusion.33
  72.3 0.1 mul.144
  72.4 0.2 select_reduce_fusion
  72.7 0.8 convolution_convert_fusion.5
  73.5 51.7 %reduce-scatter.4.cloned.1.call-done = f32[16,512]{1,0:T(8,128)} async-done(((f32[256,512]{1,0:T(8,128)}), f32[16,512]{1,0:T(8,128)}) %reduce-scatter.4.cloned.1.call-update) | async-done | bytes 32784 | tf_op jit(solution)/shard_map/reduce_scatter | solution.py:142
  125.2 0.7 fusion.52
  126.0 37.0 %all_gather.11 = bf16[256,256]{1,0:T(8,128)(2,1)S(1)} all-gather(bf16[16,256]{1,0:T(8,128)(2,1)S(1)} %fusion.52), channel_id=1, replica_groups=mesh['ep'=16,'tp'=2] {'ep'}, dimensions={0}, use_global_device_ids=true | all-gather | bytes 139264 | tf_op jit(solution)/shard_map/all_gather | solution.py:153
  163.0 0.8 convolution_convert_fusion.3
  163.8 3.5 %all-to-all-start.1 = ((bf16[16,16,128]{2,1,0:T(8,128)(2,1)}), bf16[16,16,128]{2,1,0:T(8,128)(2,1)S(1)}, u32[]{:S(2)}, u32[]{:S(2)}) async-start(bf16[16,16,128]{2,1,0:T(8,128)(2,1)} %bitcast.6), calls=%async_computation.2 | async-start | bytes 131072 | tf_op jit(solution)/shard_map/all_to_all | solution.py:157
  167.3 0.0 reduce-scatter.8.cloned.1.call-done
  167.3 2.0 %copy.73 = bf16[16,12,1024]{2,1,0:T(8,128)(2,1)} copy(bf16[16,12,1024]{2,0,1:T(8,128)(2,1)} %bitcast.128) | data formatting | bytes 786432 | tf_op jit(solution)/shard_map/reshape | solution.py:134
  169.4 5.4 %all-to-all-done.1 = bf16[16,16,128]{2,1,0:T(8,128)(2,1)S(1)} async-done(((bf16[16,16,128]{2,1,0:T(8,128)(2,1)}), bf16[16,16,128]{2,1,0:T(8,128)(2,1)S(1)}, u32[]{:S(2)}, u32[]{:S(2)}) %all-to-all-start.1) | async-done | bytes 65568 | tf_op jit(solution)/shard_map/all_to_all | solution.py:157
  174.8 3.6 %all-to-all-start.3 = ((bf16[16,12,1024]{2,1,0:T(8,128)(2,1)}), bf16[16,12,1024]{2,1,0:T(8,128)(2,1)S(1)}, u32[]{:S(2)}, u32[]{:S(2)}) async-start(bf16[16,12,1024]{2,1,0:T(8,128)(2,1)} %copy.73), calls=%async_computation.6 | async-start | bytes 1048576 | tf_op jit(solution)/shard_map/all_to_all | solution.py:135
  178.4 0.0 reduce-scatter.6.cloned.1.call-start
  178.4 0.1 copy.68
  178.5 0.8 convolution_convert_fusion.6
  179.4 0.6 copy_bitcast_fusion
  180.0 9.1 %all-to-all-done.3 = bf16[16,12,1024]{2,1,0:T(8,128)(2,1)S(1)} async-done(((bf16[16,12,1024]{2,1,0:T(8,128)(2,1)}), bf16[16,12,1024]{2,1,0:T(8,128)(2,1)S(1)}, u32[]{:S(2)}, u32[]{:S(2)}) %all-to-all-start.3) | async-done | bytes 393248 | tf_op jit(solution)/shard_map/all_to_all | solution.py:135
  189.1 0.1 reshape.246
  189.2 0.8 gather_fusion
  190.0 0.1 reshape.247
  190.0 0.2 multiply_reduce_fusion
  190.3 0.0 reduce-scatter.6.cloned.1.call-done
  190.3 1.5 add_convert_fusion
  (45 shorter events, 0.2 us)
Async XLA Ops:
  7.2 9.4 %copy-start = (bf16[512,2048]{1,0:T(8,128)(2,1)S(1)}, bf16[512,2048]{1,0:T(8,128)(2,1)}, u32[]{:S(2)}) copy-start(bf16[512,2048]{1,0:T(8,128)(2,1)} %param.31) | copy-start | bytes 6291460
  7.2 5.3 %copy-start.9 = (s32[16]{0:T(128)S(1)}, s32[16]{0:T(128)}, u32[]{:S(2)}) copy-start(s32[16]{0:T(128)} %param.23) | copy-start | bytes 196
  7.2 5.3 %copy-start.16 = (f32[8]{0:T(128)S(1)}, f32[8]{0:T(128)}, u32[]{:S(2)}) copy-start(f32[8]{0:T(128)} %param.28) | copy-start | bytes 100
  14.3 1.6 copy-start.1
  16.4 2.6 %copy-start.3 = (bf16[16,2048]{1,0:T(8,128)(2,1)S(1)}, bf16[16,2048]{1,0:T(8,128)(2,1)}, u32[]{:S(2)}) copy-start(bf16[16,2048]{1,0:T(8,128)(2,1)} %param.22) | copy-start | bytes 196612
  16.4 2.8 %copy-start.7 = (f32[2048]{0:T(1024)S(1)}, f32[2048]{0:T(1024)}, u32[]{:S(2)}) copy-start(f32[2048]{0:T(1024)} %param.32) | copy-start | bytes 24580
  16.4 2.8 %copy-start.11 = (f32[2048]{0:T(1024)S(1)}, f32[2048]{0:T(1024)}, u32[]{:S(2)}) copy-start(f32[2048]{0:T(1024)} %param.38) | copy-start | bytes 24580
  16.4 15.7 %copy-start.8 = (s32[16,6]{0,1:T(8,128)S(1)}, s32[16,6]{0,1:T(8,128)}, u32[]{:S(2)}) copy-start(s32[16,6]{0,1:T(8,128)} %param.34) | copy-start | bytes 1156
  20.0 19.6 %all-to-all-start = ((bf16[16,16,128]{2,0,1:T(8,128)(2,1)}), bf16[16,16,128]{2,0,1:T(8,128)(2,1)S(1)}, u32[]{:S(2)}, u32[]{:S(2)}) async-start(bf16[16,16,128]{2,0,1:T(8,128)(2,1)} %bitcast.106), calls=%async_computation | async-start | bytes 131072 | tf_op jit(solution)/shard_map/all_to_all | solution.py:140
  33.1 10.2 %copy-start.5 = (bf16[128,256]{1,0:T(8,128)(2,1)S(1)}, bf16[128,256]{1,0:T(8,128)(2,1)}, u32[]{:S(2)}) copy-start(bf16[128,256]{1,0:T(8,128)(2,1)} %param.36) | copy-start | bytes 196612
  33.2 10.2 %copy-start.6 = (bf16[128,256]{1,0:T(8,128)(2,1)S(1)}, bf16[128,256]{1,0:T(8,128)(2,1)}, u32[]{:S(2)}) copy-start(bf16[128,256]{1,0:T(8,128)(2,1)} %param.35) | copy-start | bytes 196612
  39.6 28.2 %all-to-all-start.2 = ((bf16[16,12,2048]{2,1,0:T(8,128)(2,1)}), bf16[16,12,2048]{2,1,0:T(8,128)(2,1)S(1)}, u32[]{:S(2)}, u32[]{:S(2)}) async-start(bf16[16,12,2048]{2,1,0:T(8,128)(2,1)} %reshape.240), calls=%async_computation.4 | async-start | bytes 2097152 | tf_op jit(solution)/shard_map/all_to_all | solution.py:129
  43.3 82.0 %reduce-scatter.4.cloned.1.call-start = ((), (), s32[]{:S(2)}) async-start(), calls=%async_computation.7 | async-start | bytes 557056 | tf_op jit(solution)/shard_map/reduce_scatter | solution.py:142
  44.4 122.9 %reduce-scatter.8.cloned.1.call-start = ((), (), s32[]{:S(2)}) async-start(), calls=%async_computation.9 | async-start | bytes 1179648 | tf_op jit(solution)/shard_map/reduce_scatter | solution.py:68
  67.8 1.8 copy-start.12
  69.5 1.2 copy-start.2
  70.8 1.3 copy-start.15
  70.8 1.9 copy-start.10
  70.8 1.9 copy-start.13
  70.8 92.2 %copy-start.4 = (bf16[256,128]{1,0:T(8,128)(2,1)S(1)}, bf16[256,128]{1,0:T(8,128)(2,1)}, u32[]{:S(2)}) copy-start(bf16[256,128]{1,0:T(8,128)(2,1)} %param.37) | copy-start | bytes 196612
  72.1 106.5 %copy-start.14 = (bf16[2048,64]{0,1:T(8,128)(2,1)S(1)}, bf16[2048,64]{0,1:T(8,128)(2,1)}, u32[]{:S(2)}) copy-start(bf16[2048,64]{0,1:T(8,128)(2,1)} %param.26) | copy-start | bytes 786436
  163.8 11.0 %all-to-all-start.1 = ((bf16[16,16,128]{2,1,0:T(8,128)(2,1)}), bf16[16,16,128]{2,1,0:T(8,128)(2,1)S(1)}, u32[]{:S(2)}, u32[]{:S(2)}) async-start(bf16[16,16,128]{2,1,0:T(8,128)(2,1)} %bitcast.6), calls=%async_computation.2 | async-start | bytes 131072 | tf_op jit(solution)/shard_map/all_to_all | solution.py:157
  174.8 14.3 %all-to-all-start.3 = ((bf16[16,12,1024]{2,1,0:T(8,128)(2,1)}), bf16[16,12,1024]{2,1,0:T(8,128)(2,1)S(1)}, u32[]{:S(2)}, u32[]{:S(2)}) async-start(bf16[16,12,1024]{2,1,0:T(8,128)(2,1)} %copy.73), calls=%async_computation.6 | async-start | bytes 1048576 | tf_op jit(solution)/shard_map/all_to_all | solution.py:135
  178.4 11.9 %reduce-scatter.6.cloned.1.call-start = ((), (), s32[]{:S(2)}) async-start(), calls=%async_computation.8 | async-start | bytes 98304 | tf_op jit(solution)/shard_map/reduce_scatter | solution.py:160
Sparse Core Ops, SparseCore 0:
  46.3 78.8 reduce-scatter.3
  127.5 4.7 reduce-scatter.7
  181.4 8.7 reduce-scatter.5
